TPU v7x, 32 devices: a whole 2x2x4 slice. The times are simulated.
32 devices in a mesh: fs: 16 (over z, y, x), tp: 2 (over core).
Axes of the slice: x: 2, y: 2, z: 4, core: 2. Of those that a mesh axis runs over, the one named last changes fastest.
Arguments:
- inputs: bfloat16 [4096, 2048], P('fs'), may hold values from -6 to 6
- query_cot: bfloat16 [4096, 1024], P('fs', 'tp'), may hold values from -0.09375 to 0.09375
- query_basis: bfloat16 [2048, 256], P('fs'), may hold values from -0.125 to 0.125
- query_master: float32 [2048, 1024], P('fs', 'tp'), may hold values from -3 to 3
- query_first: float32 [256, 1024], P('fs', 'tp'), may hold values from -4 to 4
- query_second: float32 [256, 1024], P('fs', 'tp'), may hold values from 0.02 to 4
Outputs:
- query_step: float32 [2048, 1024], P('fs', 'tp')
- query_first_new: float32 [256, 1024], P('fs', 'tp')
- query_second_new: float32 [256, 1024], P('fs', 'tp')
- query_copy: bfloat16 [2048, 1024], P('fs', 'tp')
All inputs are finite; a program needn't handle non-finite values.
Results may differ from a plain program's by a relative error of at most 0.0011.
Values may be sent and summed in bfloat16 or wider, within the bound.
A program may use at most 64 MiB of HBM per device.

v0:
```python
import jax
import jax.numpy as jnp
from jax import lax
from jax.sharding import PartitionSpec as P

HEADS = 8
DQK = 128
RANK = 256


CONTRACT = (((0,), (0,)), ((), ()))


def moments(first, second, low_grad):
    first_new = 0.8 * first + 0.2 * low_grad
    second_new = 0.9 * second + 0.1 * low_grad * low_grad
    return (first_new, second_new, first_new / jnp.sqrt(second_new))


def head_sums(update, width):
    heads_local = update.shape[1] // width
    squares = jnp.sum((update * update).reshape(-1, heads_local, width), axis=(0, 2))
    offset = lax.axis_index("tp") * heads_local
    return lax.dynamic_update_slice(jnp.zeros((HEADS,), jnp.float32), squares, (offset,))


def apply_scale(update, totals, width):
    heads_local = update.shape[1] // width
    offset = lax.axis_index("tp") * heads_local
    head_mean = lax.dynamic_slice(totals, (offset,), (heads_local,)) / (RANK * width)
    whole_mean = jnp.sum(totals) / (RANK * HEADS * width)
    factor = 1.0 / jnp.sqrt(head_mean + whole_mean)
    return (update.reshape(-1, heads_local, width) * factor[None, :, None]).reshape(update.shape)


def body(inputs, query_cot, query_basis, query_master, query_first, query_second):
    basis_q = query_basis.astype(jnp.float32)
    whole_basis = lax.all_gather(query_basis, "fs", axis=0, tiled=True)
    projected = jnp.dot(inputs, whole_basis, preferred_element_type=jnp.float32)
    partial_value = lax.dot_general(
        projected, query_cot.astype(jnp.float32), CONTRACT, precision=lax.Precision.HIGHEST
    )
    low_parts = lax.psum_scatter(partial_value, "fs", scatter_dimension=0, tiled=True)
    first_q, second_q, update_q = moments(query_first, query_second, low_parts)
    totals_q = lax.psum(head_sums(update_q, DQK), ("fs", "tp"))
    scaled_q = apply_scale(update_q, totals_q, DQK)
    gathered_q = lax.all_gather(scaled_q, "fs", axis=0, tiled=True)
    step_q = jnp.dot(basis_q, gathered_q, precision=lax.Precision.HIGHEST)
    copy_q = (query_master + step_q).astype(jnp.bfloat16)
    return (step_q, first_q, second_q, copy_q)


def solution(mesh):
    placed = (
        P("fs", None),
        P("fs", "tp"),
        P("fs", None),
        P("fs", "tp"),
        P("fs", "tp"),
        P("fs", "tp"),
    )
    return jax.shard_map(
        body,
        mesh=mesh,
        in_specs=placed,
        out_specs=(P("fs", "tp"), P("fs", "tp"), P("fs", "tp"), P("fs", "tp")),
        check_vma=False,
    )
```

profile of v0, /device:TPU:0, one launch (start us, length us, event | category | flops | bytes accessed | tf_op | source)
XLA Modules:
  0.0 238.5 jit_solution(4962275286878473010)
XLA Ops:
  7.2 0.0 copy-start
  7.2 0.0 all-gather.2.cloned.1.call-start
  7.2 0.7 all-gather.2.cloned.1.call-update
  7.9 0.0 copy-start.3
  7.9 0.0 reduce-scatter.2.cloned.1.call-start
  8.0 60.6 %all-gather.2.cloned.1.call-done = bf16[2048,256]{1,0:T(8,128)(2,1)} async-done(((bf16[128,256]{1,0:T(8,128)(2,1)}), bf16[2048,256]{1,0:T(8,128)(2,1)}) %all-gather.2.cloned.1.call-update) | async-done | bytes 1048592 | tf_op jit(solution)/shard_map/all_gather | solution.py:38
  68.6 0.0 copy-done
  68.6 1.7 fusion.2
  70.3 0.0 copy-done.3
  70.3 1.2 fusion.3
  71.5 0.0 copy-start.6
  71.5 0.0 copy-start.7
  71.5 0.0 copy-start.2
  71.5 0.0 reduce-scatter.2.cloned.1.call-update
  71.5 76.4 %reduce-scatter.2.cloned.1.call-done = f32[16,512]{1,0:T(8,128)} async-done(((f32[256,512]{1,0:T(8,128)}), f32[16,512]{1,0:T(8,128)}) %reduce-scatter.2.cloned.1.call-update) | async-done | bytes 32784 | tf_op jit(solution)/shard_map/reduce_scatter | solution.py:43
  147.9 0.0 copy-done.6
  148.0 0.0 copy-done.7
  148.0 0.8 multiply_reduce_fusion
  148.7 0.0 copy-start.4
  148.8 0.0 copy-start.5
  148.8 0.1 bitcast_reduce_fusion
  148.9 0.2 dynamic_update_slice.3
  149.1 0.0 copy-done.2
  149.1 0.1 copy.13
  149.3 36.8 %psum.7 = f32[8]{0:T(128)S(1)} all-reduce(f32[8]{0:T(128)S(1)} %dynamic_update_slice.3), channel_id=1, replica_groups=mesh['fs'=16,'tp'=2] {'fs','tp'}, use_global_device_ids=true, to_apply=%region_3.0 | all-reduce | flops 8 | bytes 64 | tf_op jit(solution)/shard_map/psum | solution.py:45
  186.1 0.6 reduce_sum.28
  187.4 0.1 add_rsqrt_fusion
  187.4 0.1 broadcast_bitcast_fusion
  187.5 0.0 copy-done.4
  187.5 0.0 copy-done.5
  187.5 0.0 copy-start.1
  187.6 41.9 %all_gather.7 = f32[256,512]{1,0:T(8,128)S(1)} all-gather(f32[16,512]{1,0:T(8,128)S(1)} %broadcast_multiply_fusion), channel_id=1, replica_groups=mesh['fs'=16,'tp'=2] {'fs'}, dimensions={0}, use_global_device_ids=true | all-gather | bytes 557056 | tf_op jit(solution)/shard_map/all_gather | solution.py:47
  229.4 0.0 copy-done.1
  229.4 0.6 add_convert_fusion
  230.1 0.8 copy.15
  230.8 0.8 copy.14
  (2 shorter events, 0.0 us)
Async XLA Ops:
  7.2 61.4 %copy-start = (bf16[256,2048]{1,0:T(8,128)(2,1)S(1)}, bf16[256,2048]{1,0:T(8,128)(2,1)}, u32[]{:S(2)}) copy-start(bf16[256,2048]{1,0:T(8,128)(2,1)} %param.6) | copy-start | bytes 3145732
  7.2 61.4 %all-gather.2.cloned.1.call-start = ((), (), s32[]{:S(2)}) async-start(), calls=%async_computation.1 | async-start | bytes 1114112 | tf_op jit(solution)/shard_map/all_gather | solution.py:38
  7.9 62.3 %copy-start.3 = (bf16[256,512]{1,0:T(8,128)(2,1)S(1)}, bf16[256,512]{1,0:T(8,128)(2,1)}, u32[]{:S(2)}) copy-start(bf16[256,512]{1,0:T(8,128)(2,1)} %param.7) | copy-start | bytes 786436
  7.9 140.0 %reduce-scatter.2.cloned.1.call-start = ((), (), s32[]{:S(2)}) async-start(), calls=%async_computation.2 | async-start | bytes 557056 | tf_op jit(solution)/shard_map/reduce_scatter | solution.py:43
  71.5 76.5 %copy-start.6 = (f32[16,512]{1,0:T(8,128)S(1)}, f32[16,512]{1,0:T(8,128)}, u32[]{:S(2)}) copy-start(f32[16,512]{1,0:T(8,128)} %param.11) | copy-start | bytes 98308
  71.5 76.5 %copy-start.7 = (f32[16,512]{1,0:T(8,128)S(1)}, f32[16,512]{1,0:T(8,128)}, u32[]{:S(2)}) copy-start(f32[16,512]{1,0:T(8,128)} %param.10) | copy-start | bytes 98308
  71.5 77.6 %copy-start.2 = (f32[128,512]{1,0:T(8,128)S(1)}, f32[128,512]{1,0:T(8,128)}, u32[]{:S(2)}) copy-start(f32[128,512]{1,0:T(8,128)} %param.9) | copy-start | bytes 786436
  148.7 38.8 %copy-start.4 = (f32[16,512]{1,0:T(8,128)}, f32[16,512]{1,0:T(8,128)S(1)}, u32[]{:S(2)}) copy-start(f32[16,512]{1,0:T(8,128)S(1)} %get-tuple-element.13) | copy-start | bytes 98308
  148.8 38.8 %copy-start.5 = (f32[16,512]{1,0:T(8,128)}, f32[16,512]{1,0:T(8,128)S(1)}, u32[]{:S(2)}) copy-start(f32[16,512]{1,0:T(8,128)S(1)} %get-tuple-element.14) | copy-start | bytes 98308
  187.5 41.9 %copy-start.1 = (bf16[128,256]{1,0:T(8,128)(2,1)S(1)}, bf16[128,256]{1,0:T(8,128)(2,1)}, u32[]{:S(2)}) copy-start(bf16[128,256]{1,0:T(8,128)(2,1)} %param.8) | copy-start | bytes 196612
Sparse Core Ops, SparseCore 0:
  10.7 57.7 all-gather.1
  71.6 76.2 reduce-scatter.1
where the time goes:
time: 239 us
  waiting for transfers between devices  138 us (58%)
  blocking collectives  78.7 us (33%)
  between operations  14.8 us (6%)
  matrix products  3.48 us (1%)
    reduce_scatter x1, waiting for transfers between devices, body(): lax.psum_scatter(partial_value, 'fs', scatter_dimension=0, tiled=True)  76.4 us
    all_gather x1, waiting for transfers between devices, body(): whole_basis = lax.all_gather(query_basis, 'fs', axis=0, tiled=True)  60.6 us
    all_gather x1, blocking collectives, body(): gathered_q = lax.all_gather(scaled_q, 'fs', axis=0, tiled=True)  41.9 us
    psum x1, blocking collectives, body(): totals_q = lax.psum(head_sums(update_q, DQK), ('fs', 'tp'))  36.8 us
  transfers between devices with their start and end apart: 2, of which 2 were waited for; matrix products, arithmetic and copies ran while one was open for 0% of the time, Pallas kernels for 0%

commit v1 on v0

v1 whole, which is shorter than its diff:
```python
import functools

import jax
import jax.numpy as jnp
from jax import lax
from jax.experimental import pallas as pl
from jax.experimental.pallas import tpu as pltpu
from jax.sharding import PartitionSpec as P

DQK = 128
MESH = pl.DeviceIdType.MESH
CONTRACT = (((0,), (0,)), ((), ()))


def split2(value):
    high = value.astype(jnp.bfloat16)
    low = (value - high.astype(jnp.float32)).astype(jnp.bfloat16)
    return high, low


def kernel(
    n, nz, nq, tp,
    inputs_ref, cot_ref, basis_ref, master_ref, first_ref, second_ref,
    step_ref, first_out, second_out, copy_ref,
    xv, cv, mv, ball, pbuf, part, rbuf, zsend, zbuf, ubuf, ufull, sums,
    load_sem, b_send, b_recv, p_send, p_recv, r_send, r_recv, z_send, z_recv,
    u_send, u_recv, s_send, s_recv,
):
    me = lax.axis_index("fs")
    t = lax.axis_index("tp")
    z, q = me // nq, me % nq
    half = t % 2
    partner = t + 1 - 2 * half
    rank_half = ball.shape[2]
    rr, cols = first_ref.shape
    rank = rr * n
    nzh = nz // 2

    def remote(src, dst, send, recv, fs, core):
        return pltpu.make_async_remote_copy(
            src_ref=src, dst_ref=dst, send_sem=send, recv_sem=recv,
            device_id=(fs, core), device_id_type=MESH,
        )

    loads = [
        pltpu.make_async_copy(inputs_ref, xv, load_sem.at[0]),
        pltpu.make_async_copy(cot_ref, cv, load_sem.at[1]),
        pltpu.make_async_copy(master_ref, mv, load_sem.at[2]),
    ]
    for load in loads:
        load.start()

    barrier = pltpu.get_barrier_semaphore()
    for d in range(1, nz):
        pl.semaphore_signal(barrier, inc=1, device_id=((z + d) % nz * nq + q, t), device_id_type=MESH)
    for d in range(1, nq):
        pl.semaphore_signal(barrier, inc=1, device_id=(z * nq + (q + d) % nq, t), device_id_type=MESH)
    for d in range(1, tp):
        pl.semaphore_signal(barrier, inc=1, device_id=(me, (t + d) % tp), device_id_type=MESH)
    pl.semaphore_wait(barrier, nz - 1 + nq - 1 + tp - 1)

    def gather(own, buf, send, recv):
        started = []
        for d in range(1, nz):
            copy = remote(own, buf.at[me], send.at[d], recv.at[me], (z + d) % nz * nq + q, t)
            copy.start()
            started.append(copy)
        for k in range(nz):
            c = (z + k) % nz * nq + q
            if k > 0:
                remote(own, buf.at[c], send.at[0], recv.at[c], me, t).wait_recv()
            source = own if k == 0 else buf.at[c]
            for d in range(1, nq):
                copy = remote(
                    source, buf.at[c], send.at[nz + k * nq + d], recv.at[c], z * nq + (q + d) % nq, t
                )
                copy.start()
                started.append(copy)
        for k in range(nz):
            for d in range(1, nq):
                c = (z + k) % nz * nq + (q + d) % nq
                remote(own, buf.at[c], send.at[0], recv.at[c], me, t).wait_recv()
        return started

    started = []
    own_basis = basis_ref.at[:, pl.ds(pl.multiple_of(half * rank_half, rank_half), rank_half)]
    mine = pltpu.make_async_copy(own_basis, ball.at[me], load_sem.at[3])
    mine.start()
    mine.wait()
    started += gather(ball.at[me], ball, b_send, b_recv)

    loads[0].wait()
    pbuf[half] = jnp.dot(
        xv[...], ball[...].reshape(xv.shape[1], rank_half), preferred_element_type=jnp.float32
    )
    swap = remote(pbuf.at[half], pbuf.at[half], p_send, p_recv, me, partner)
    swap.start()
    started.append(swap)
    loads[1].wait()

    def shares(hh, slot):
        high, low = split2(pbuf[hh])
        value = lax.dot_general(high, cv[...], CONTRACT, preferred_element_type=jnp.float32)
        value += lax.dot_general(low, cv[...], CONTRACT, preferred_element_type=jnp.float32)
        for k in range(nzh):
            for j in range(nq):
                at = (k * nq + j) * rr
                part[j, hh * nzh + k] = value[at : at + rr].astype(part.dtype)
        for d in range(1, nq):
            to = (q + d) % nq
            copy = remote(
                part.at[to, pl.ds(hh * nzh, nzh)], rbuf.at[q, pl.ds(hh * nzh, nzh)],
                r_send.at[slot, d], r_recv.at[slot, q], z * nq + to, t,
            )
            copy.start()
            started.append(copy)

    def combine(hh, slot):
        for d in range(1, nq):
            j = (q + d) % nq
            remote(
                part.at[j, pl.ds(hh * nzh, nzh)], rbuf.at[j, pl.ds(hh * nzh, nzh)],
                r_send.at[slot, 0], r_recv.at[slot, j], me, t,
            ).wait_recv()
        for k in range(nzh):
            zz = hh * nzh + k
            total = part[q, zz].astype(jnp.float32)
            for d in range(1, nq):
                total += rbuf[(q + d) % nq, zz].astype(jnp.float32)
            zsend[zz] = total

            @pl.when(zz != z)
            def _():
                remote(
                    zsend.at[zz], zbuf.at[z], z_send.at[zz], z_recv.at[z], zz * nq + q, t
                ).start()

    other = 1 - half
    shares(half, 0)
    remote(pbuf.at[other], pbuf.at[other], p_send, p_recv, me, partner).wait_recv()
    shares(other, 1)
    combine(half, 0)
    combine(other, 1)
    low = zsend[z]
    for d in range(1, nz):
        zz = (z + d) % nz
        remote(zsend.at[z], zbuf.at[zz], z_send.at[zz], z_recv.at[zz], me, t).wait_recv()
        low += zbuf[zz]

    first_new = 0.8 * first_ref[...] + 0.2 * low
    second_new = 0.9 * second_ref[...] + 0.1 * low * low
    ubuf[me] = first_new / jnp.sqrt(second_new)
    first_out[...] = first_new
    second_out[...] = second_new
    started += gather(ubuf.at[me], ubuf, u_send, u_recv)

    if rr % 8 == 0:
        update = ubuf[...].reshape(rank, cols)
    else:
        for i in range(n):
            ufull[i * rr : (i + 1) * rr, :] = ubuf[i]
        update = ufull[...]
    squares = jnp.sum(update * update, axis=0, keepdims=True)
    total = jnp.sum(squares, axis=1, keepdims=True)
    sums[t] = jnp.broadcast_to(total, sums.shape[1:])
    for d in range(1, tp):
        copy = remote(sums.at[t], sums.at[t], s_send.at[d], s_recv.at[t], me, (t + d) % tp)
        copy.start()
        started.append(copy)

    high, low_bits = split2(update)
    step = jnp.dot(basis_ref[...], high, preferred_element_type=jnp.float32)
    step += jnp.dot(basis_ref[...], low_bits, preferred_element_type=jnp.float32)

    whole = sums[t][:1]
    for d in range(1, tp):
        c = (t + d) % tp
        remote(sums.at[c], sums.at[c], s_send.at[d], s_recv.at[c], me, c).wait_recv()
        whole += sums[c][:1]
    whole = whole / (rank * cols * tp)
    loads[2].wait()
    for i in range(cols // DQK):
        at = slice(i * DQK, (i + 1) * DQK)
        head = jnp.sum(squares[:, at], axis=1, keepdims=True) / (rank * DQK)
        factor = 1.0 / jnp.sqrt(head + whole)
        block = step[:, at] * factor
        step_ref[:, at] = block
        copy_ref[:, at] = (mv[:, at] + block).astype(jnp.bfloat16)

    for copy in started:
        copy.wait_send()
    for d in range(1, nz):
        zz = (z + d) % nz
        remote(zsend.at[zz], zbuf.at[z], z_send.at[zz], z_recv.at[z], zz * nq + q, t).wait_send()


def body(n, tp, inputs, query_cot, query_basis, query_master, query_first, query_second):
    nq = 1
    while nq * nq < n:
        nq *= 2
    nz = n // nq
    tokens, width = inputs.shape
    rows, rank = query_basis.shape
    rr, cols = query_first.shape
    f32, bf16 = jnp.float32, jnp.bfloat16
    dma = pltpu.SemaphoreType.DMA
    vmem = pl.BlockSpec(memory_space=pltpu.VMEM)
    hbm = pl.BlockSpec(memory_space=pl.ANY)
    return pl.pallas_call(
        functools.partial(kernel, n, nz, nq, tp),
        out_shape=(
            jax.ShapeDtypeStruct((rows, cols), f32),
            jax.ShapeDtypeStruct((rr, cols), f32),
            jax.ShapeDtypeStruct((rr, cols), f32),
            jax.ShapeDtypeStruct((rows, cols), bf16),
        ),
        in_specs=[hbm, hbm, vmem, hbm, vmem, vmem],
        out_specs=(vmem,) * 4,
        scratch_shapes=[
            pltpu.VMEM((tokens, width), bf16),
            pltpu.VMEM((tokens, cols), bf16),
            pltpu.VMEM((rows, cols), f32),
            pltpu.VMEM((n, rows, rank // 2), bf16),
            pltpu.VMEM((2, tokens, rank // 2), f32),
            pltpu.VMEM((nq, nz, rr, cols), f32),
            pltpu.VMEM((nq, nz, rr, cols), f32),
            pltpu.VMEM((nz, rr, cols), f32),
            pltpu.VMEM((nz, rr, cols), f32),
            pltpu.VMEM((n, rr, cols), f32),
            pltpu.VMEM((rank, cols), f32),
            pltpu.VMEM((tp, 8, 128), f32),
            dma((4,)),
            dma((nz + n,)), dma((n,)),
            dma, dma,
            dma((2, nq)), dma((2, nq)),
            dma((nz,)), dma((nz,)),
            dma((nz + n,)), dma((n,)),
            dma((tp,)), dma((tp,)),
        ],
        compiler_params=pltpu.CompilerParams(collective_id=0, has_side_effects=True),
    )(inputs, query_cot, query_basis, query_master, query_first, query_second)


def solution(mesh):
    placed = (
        P("fs", None),
        P("fs", "tp"),
        P("fs", None),
        P("fs", "tp"),
        P("fs", "tp"),
        P("fs", "tp"),
    )
    return jax.shard_map(
        functools.partial(body, mesh.shape["fs"], mesh.shape["tp"]),
        mesh=mesh,
        in_specs=placed,
        out_specs=(P("fs", "tp"),) * 4,
        check_vma=False,
    )
```

time: 239 us -> 43 us (0.18)
  waiting for transfers between devices: 138 us -> 0 us
  blocking collectives: 78.7 us -> 0 us
  Pallas kernels: 0 us -> 38.3 us
  between operations: 14.8 us -> 0.66 us
  matrix products: 3.48 us -> 0 us
    reduce_scatter x1 -> x0, waiting for transfers between devices: 76.4 us -> none  [body(): lax.psum_scatter(partial_value, 'fs', scatter_dimension=0, tiled=True)]
    all_gather x1 -> x0, waiting for transfers between devices: 60.6 us -> none  [body(): whole_basis = lax.all_gather(query_basis, 'fs', axis=0, tiled=True)]
    all_gather x1 -> x0, blocking collectives: 41.9 us -> none  [body(): gathered_q = lax.all_gather(scaled_q, 'fs', axis=0, tiled=True)]
    pallas_call x0 -> x1, Pallas kernels: none -> 38.3 us  [body(): pl.pallas_call(functools.partial(kernel, n, nz, nq, tp), out_shape=(jax.S...]
    psum x1 -> x0, blocking collectives: 36.8 us -> none  [body(): totals_q = lax.psum(head_sums(update_q, DQK), ('fs', 'tp'))]
    dot_general x3 -> x0, matrix products: 3.48 us -> none  [the longest x1 1.66 us: body(): projected = jnp.dot(inputs, whole_basis, preferred_element_type=jnp.float32)]
  transfers between devices with their start and end apart: 2 -> 0, of which waited for: 2 -> 0; matrix products, arithmetic and copies ran while one was open for 0% -> 0% of each run, Pallas kernels for 0% -> 0%
where the time goes in v1:
time: 43 us; the launch traced here: 42.7 us
  Pallas kernels  38.3 us (89%)
  local copies, waits for them, and re-layouts  3.76 us (9%)
  between operations  0.66 us (2%)
    pallas_call x1, Pallas kernels, body(): pl.pallas_call(functools.partial(kernel, n, nz, nq, tp), out_shape=(jax.S...  38.3 us
    unnamed x10, local copies, waits for them, and re-layouts  3.76 us

profile of v1, /device:TPU:0, one launch (start us, length us, event | category | flops | bytes accessed | tf_op | source)
XLA Modules:
  0.0 42.7 jit_solution(9359522886900252732)
XLA Ops:
  0.6 38.3 %shard_map.93 = (f32[128,512]{1,0:T(8,128)}, f32[16,512]{1,0:T(8,128)}, f32[16,512]{1,0:T(8,128)}, bf16[128,512]{1,0:T(8,128)(2,1)}) custom-call(bf16[256,2048]{1,0:T(8,128)(2,1)} %inputs_ref.1, bf16[256,512]{1,0:T(8,128)(2,1)} %cot_ref.1, bf16[128,256]{1,0:T(8,128)(2,1)} %basis_ref.1, f32[128,512]{1,0:T(8,128)} %master_ref.1, f32[16,512]{1,0:T(8,128)} %first_ref.1, ...), custom_call_target="tpu_custom_call" | custom-call | tf_op jit(solution)/shard_map/pallas_call | solution.py:209
  38.9 0.0 copy-start.2
  38.9 0.0 copy-start
  39.0 1.7 %copy.14 = f32[128,512]{1,0:T(8,128)} copy(f32[128,512]{1,0:T(8,128)} %get-tuple-element.8) | data formatting | bytes 524288
  40.7 0.0 copy-done.2
  40.7 0.0 copy-start.1
  40.7 0.6 %copy.15 = f32[16,512]{1,0:T(8,128)} copy(f32[16,512]{1,0:T(8,128)S(1)} %copy-done.2) | data formatting | bytes 65536
  41.3 0.2 copy-done.1
  41.4 0.6 %copy.16 = f32[16,512]{1,0:T(8,128)} copy(f32[16,512]{1,0:T(8,128)S(1)} %copy-done.1) | data formatting | bytes 65536
  42.1 0.0 copy-done
  42.1 0.7 %copy.17 = bf16[128,512]{1,0:T(8,128)(2,1)} copy(bf16[128,512]{1,0:T(8,128)(2,1)S(1)} %copy-done) | data formatting | bytes 262144
Async XLA Ops:
  38.9 1.7 %copy-start.2 = (f32[16,512]{1,0:T(8,128)S(1)}, f32[16,512]{1,0:T(8,128)}, u32[]{:S(2)}) copy-start(f32[16,512]{1,0:T(8,128)} %get-tuple-element.9) | copy-start | bytes 98308
  38.9 3.1 %copy-start = (bf16[128,512]{1,0:T(8,128)(2,1)S(1)}, bf16[128,512]{1,0:T(8,128)(2,1)}, u32[]{:S(2)}) copy-start(bf16[128,512]{1,0:T(8,128)(2,1)} %get-tuple-element.11) | copy-start | bytes 393220
  40.7 0.8 %copy-start.1 = (f32[16,512]{1,0:T(8,128)S(1)}, f32[16,512]{1,0:T(8,128)}, u32[]{:S(2)}) copy-start(f32[16,512]{1,0:T(8,128)} %get-tuple-element.10) | copy-start | bytes 98308

commit v2 on v1

--- a/solution.py
+++ b/solution.py
@@ -18,11 +18,15 @@
     return high, low
 
 
+def moments(first, second, low):
+    return 0.8 * first + 0.2 * low, 0.9 * second + 0.1 * low * low
+
+
 def kernel(
     n, nz, nq, tp,
-    inputs_ref, cot_ref, basis_ref, master_ref, first_ref, second_ref,
-    step_ref, first_out, second_out, copy_ref,
-    xv, cv, mv, ball, pbuf, part, rbuf, zsend, zbuf, ubuf, ufull, sums,
+    inputs_ref, cot_ref, basis_ref, first_ref, second_ref,
+    product_ref, factor_ref, low_ref,
+    xv, cv, bv, fv, sv, ball, pbuf, part, rbuf, zsend, zbuf, ubuf, ufull, sums,
     load_sem, b_send, b_recv, p_send, p_recv, r_send, r_recv, z_send, z_recv,
     u_send, u_recv, s_send, s_recv,
 ):
@@ -42,13 +46,15 @@
             device_id=(fs, core), device_id_type=MESH,
         )
 
+    own_basis = basis_ref.at[:, pl.ds(pl.multiple_of(half * rank_half, rank_half), rank_half)]
     loads = [
-        pltpu.make_async_copy(inputs_ref, xv, load_sem.at[0]),
-        pltpu.make_async_copy(cot_ref, cv, load_sem.at[1]),
-        pltpu.make_async_copy(master_ref, mv, load_sem.at[2]),
+        pltpu.make_async_copy(own_basis, ball.at[me], load_sem.at[0]),
+        pltpu.make_async_copy(inputs_ref, xv, load_sem.at[1]),
+        pltpu.make_async_copy(cot_ref, cv, load_sem.at[2]),
+        pltpu.make_async_copy(first_ref, fv, load_sem.at[3]),
+        pltpu.make_async_copy(second_ref, sv, load_sem.at[4]),
+        pltpu.make_async_copy(basis_ref, bv, load_sem.at[5]),
     ]
-    for load in loads:
-        load.start()
 
     barrier = pltpu.get_barrier_semaphore()
     for d in range(1, nz):
@@ -57,6 +63,8 @@
         pl.semaphore_signal(barrier, inc=1, device_id=(z * nq + (q + d) % nq, t), device_id_type=MESH)
     for d in range(1, tp):
         pl.semaphore_signal(barrier, inc=1, device_id=(me, (t + d) % tp), device_id_type=MESH)
+    for load in loads:
+        load.start()
     pl.semaphore_wait(barrier, nz - 1 + nq - 1 + tp - 1)
 
     def gather(own, buf, send, recv):
@@ -83,20 +91,17 @@
         return started
 
     started = []
-    own_basis = basis_ref.at[:, pl.ds(pl.multiple_of(half * rank_half, rank_half), rank_half)]
-    mine = pltpu.make_async_copy(own_basis, ball.at[me], load_sem.at[3])
-    mine.start()
-    mine.wait()
+    loads[0].wait()
     started += gather(ball.at[me], ball, b_send, b_recv)
 
-    loads[0].wait()
+    loads[1].wait()
     pbuf[half] = jnp.dot(
         xv[...], ball[...].reshape(xv.shape[1], rank_half), preferred_element_type=jnp.float32
     )
     swap = remote(pbuf.at[half], pbuf.at[half], p_send, p_recv, me, partner)
     swap.start()
     started.append(swap)
-    loads[1].wait()
+    loads[2].wait()
 
     def shares(hh, slot):
         high, low = split2(pbuf[hh])
@@ -147,11 +152,11 @@
         remote(zsend.at[z], zbuf.at[zz], z_send.at[zz], z_recv.at[zz], me, t).wait_recv()
         low += zbuf[zz]
 
-    first_new = 0.8 * first_ref[...] + 0.2 * low
-    second_new = 0.9 * second_ref[...] + 0.1 * low * low
+    for load in loads[3:]:
+        load.wait()
+    first_new, second_new = moments(fv[...], sv[...], low)
     ubuf[me] = first_new / jnp.sqrt(second_new)
-    first_out[...] = first_new
-    second_out[...] = second_new
+    low_ref[...] = low
     started += gather(ubuf.at[me], ubuf, u_send, u_recv)
 
     if rr % 8 == 0:
@@ -169,8 +174,9 @@
         started.append(copy)
 
     high, low_bits = split2(update)
-    step = jnp.dot(basis_ref[...], high, preferred_element_type=jnp.float32)
-    step += jnp.dot(basis_ref[...], low_bits, preferred_element_type=jnp.float32)
+    product = jnp.dot(bv[...], high, preferred_element_type=jnp.float32)
+    product += jnp.dot(bv[...], low_bits, preferred_element_type=jnp.float32)
+    product_ref[...] = product
 
     whole = sums[t][:1]
     for d in range(1, tp):
@@ -178,20 +184,27 @@
         remote(sums.at[c], sums.at[c], s_send.at[d], s_recv.at[c], me, c).wait_recv()
         whole += sums[c][:1]
     whole = whole / (rank * cols * tp)
-    loads[2].wait()
     for i in range(cols // DQK):
         at = slice(i * DQK, (i + 1) * DQK)
         head = jnp.sum(squares[:, at], axis=1, keepdims=True) / (rank * DQK)
         factor = 1.0 / jnp.sqrt(head + whole)
-        block = step[:, at] * factor
-        step_ref[:, at] = block
-        copy_ref[:, at] = (mv[:, at] + block).astype(jnp.bfloat16)
+        factor_ref[:, at] = jnp.broadcast_to(factor, (factor_ref.shape[0], DQK))
 
     for copy in started:
         copy.wait_send()
     for d in range(1, nz):
         zz = (z + d) % nz
         remote(zsend.at[zz], zbuf.at[z], z_send.at[zz], z_recv.at[z], zz * nq + q, t).wait_send()
+
+
+def finish(
+    product_ref, factor_ref, low_ref, first_ref, second_ref, master_ref,
+    step_ref, first_out, second_out, copy_ref,
+):
+    first_out[...], second_out[...] = moments(first_ref[...], second_ref[...], low_ref[...])
+    step = product_ref[...] * factor_ref[:1]
+    step_ref[...] = step
+    copy_ref[...] = (master_ref[...] + step).astype(jnp.bfloat16)
 
 
 def body(n, tp, inputs, query_cot, query_basis, query_master, query_first, query_second):
@@ -206,20 +219,21 @@
     dma = pltpu.SemaphoreType.DMA
     vmem = pl.BlockSpec(memory_space=pltpu.VMEM)
     hbm = pl.BlockSpec(memory_space=pl.ANY)
-    return pl.pallas_call(
+    product, factor, low = pl.pallas_call(
         functools.partial(kernel, n, nz, nq, tp),
         out_shape=(
             jax.ShapeDtypeStruct((rows, cols), f32),
+            jax.ShapeDtypeStruct((8, cols), f32),
             jax.ShapeDtypeStruct((rr, cols), f32),
-            jax.ShapeDtypeStruct((rr, cols), f32),
-            jax.ShapeDtypeStruct((rows, cols), bf16),
         ),
-        in_specs=[hbm, hbm, vmem, hbm, vmem, vmem],
-        out_specs=(vmem,) * 4,
+        in_specs=[hbm] * 5,
+        out_specs=(vmem,) * 3,
         scratch_shapes=[
             pltpu.VMEM((tokens, width), bf16),
             pltpu.VMEM((tokens, cols), bf16),
-            pltpu.VMEM((rows, cols), f32),
+            pltpu.VMEM((rows, rank), bf16),
+            pltpu.VMEM((rr, cols), f32),
+            pltpu.VMEM((rr, cols), f32),
             pltpu.VMEM((n, rows, rank // 2), bf16),
             pltpu.VMEM((2, tokens, rank // 2), f32),
             pltpu.VMEM((nq, nz, rr, cols), f32),
@@ -229,7 +243,7 @@
             pltpu.VMEM((n, rr, cols), f32),
             pltpu.VMEM((rank, cols), f32),
             pltpu.VMEM((tp, 8, 128), f32),
-            dma((4,)),
+            dma((6,)),
             dma((nz + n,)), dma((n,)),
             dma, dma,
             dma((2, nq)), dma((2, nq)),
@@ -238,7 +252,18 @@
             dma((tp,)), dma((tp,)),
         ],
         compiler_params=pltpu.CompilerParams(collective_id=0, has_side_effects=True),
-    )(inputs, query_cot, query_basis, query_master, query_first, query_second)
+    )(inputs, query_cot, query_basis, query_first, query_second)
+    return pl.pallas_call(
+        finish,
+        out_shape=(
+            jax.ShapeDtypeStruct((rows, cols), f32),
+            jax.ShapeDtypeStruct((rr, cols), f32),
+            jax.ShapeDtypeStruct((rr, cols), f32),
+            jax.ShapeDtypeStruct((rows, cols), bf16),
+        ),
+        in_specs=[vmem] * 6,
+        out_specs=(vmem,) * 4,
+    )(product, factor, low, query_first, query_second, query_master)
 
 
 def solution(mesh):

time: 43 us -> 39.8 us (0.926)
  local copies, waits for them, and re-layouts: 3.76 us -> 0 us
  Pallas kernels: 38.3 us -> 38.9 us
    unnamed x10 -> x0, local copies, waits for them, and re-layouts: 3.76 us -> none
    pallas_call x0 -> x1, Pallas kernels: none -> 1.88 us  [body(): pl.pallas_call(finish, out_shape=(jax.ShapeDtypeStruct((rows, cols), f32)...]
    pallas_call x1, Pallas kernels: 38.3 us -> 37 us  [body(): pl.pallas_call(functools.partial(kernel, n, nz, nq, tp), out_shape=(jax.S...]
where the time goes in v2:
time: 39.8 us; the launch traced here: 39.5 us
  Pallas kernels  38.9 us (98%)
  between operations  0.64 us (2%)
    pallas_call x1, Pallas kernels, body(): pl.pallas_call(functools.partial(kernel, n, nz, nq, tp), out_shape=(jax.S...  37 us
    pallas_call x1, Pallas kernels, body(): pl.pallas_call(finish, out_shape=(jax.ShapeDtypeStruct((rows, cols), f32)...  1.88 us

profile of v2, /device:TPU:0, one launch (start us, length us, event | category | flops | bytes accessed | tf_op | source)
XLA Modules:
  0.0 39.5 jit_solution(1003019886773556844)
XLA Ops:
  0.6 37.0 %shard_map.93 = (f32[128,512]{1,0:T(8,128)}, f32[8,512]{1,0:T(8,128)}, f32[16,512]{1,0:T(8,128)}) custom-call(bf16[256,2048]{1,0:T(8,128)(2,1)} %inputs_ref.1, bf16[256,512]{1,0:T(8,128)(2,1)} %cot_ref.1, bf16[128,256]{1,0:T(8,128)(2,1)} %basis_ref.1, f32[16,512]{1,0:T(8,128)} %first_ref.3, f32[16,512]{1,0:T(8,128)} %second_ref.3), custom_call_target="tpu_custom_call" | custom-call | tf_op jit(solution)/shard_map/pallas_call | solution.py:222
  37.7 1.9 %shard_map.94 = (f32[128,512]{1,0:T(8,128)}, f32[16,512]{1,0:T(8,128)}, f32[16,512]{1,0:T(8,128)}, bf16[128,512]{1,0:T(8,128)(2,1)}) custom-call(f32[128,512]{1,0:T(8,128)} %get-tuple-element.7.product_ref, f32[8,512]{1,0:T(8,128)} %get-tuple-element.8.factor_ref, f32[16,512]{1,0:T(8,128)} %get-tuple-element.9.low_ref, f32[16,512]{1,0:T(8,128)} %first_ref.3, ...), custom_call_target="tpu_custom_call" | custom-call | tf_op jit(solution)/shard_map/pallas_call | solution.py:256

commit v3 on v2

v3 whole, which is shorter than its diff:
```python
import functools

import jax
import jax.numpy as jnp
from jax import lax
from jax.experimental import pallas as pl
from jax.experimental.pallas import tpu as pltpu
from jax.sharding import PartitionSpec as P

DQK = 128
MESH = pl.DeviceIdType.MESH
CONTRACT = (((0,), (0,)), ((), ()))


def split2(value):
    high = value.astype(jnp.bfloat16)
    low = (value - high.astype(jnp.float32)).astype(jnp.bfloat16)
    return high, low


def moments(first, second, low):
    return 0.8 * first + 0.2 * low, 0.9 * second + 0.1 * low * low


def kernel(
    n, na, nb, nz, tp, groups,
    inputs_ref, cot_ref, basis_ref, first_ref, second_ref,
    product_ref, factor_ref, low_ref,
    xv, cv, bv, fv, sv, ball, pbuf, part, rbuf, zsend, zbuf, ubuf, ufull, sums,
    load_sem, send_sem, p_recv, b_recv, r_recv, z_send, z_recv, u_recv, s_recv,
):
    me = lax.axis_index("fs")
    t = lax.axis_index("tp")
    nq = na * nb
    z, q = me // nq, me % nq
    a, b = q // nb, q % nb
    half = t % 2
    partner = t + 1 - 2 * half
    rank_half = bv.shape[1] // 2
    rows = bv.shape[0]
    rr, cols = first_ref.shape
    rank = rr * n
    nzh = nz // 2
    width = cols // groups
    started = []

    def remote(src, dst, send, recv, fs, core):
        return pltpu.make_async_remote_copy(
            src_ref=src, dst_ref=dst, send_sem=send, recv_sem=recv,
            device_id=(fs, core), device_id_type=MESH,
        )

    def send(src, dst, recv, fs, core):
        copy = remote(src, dst, send_sem.at[len(started)], recv, fs, core)
        copy.start()
        started.append(copy)

    def arrive(dst, recv):
        remote(dst, dst, send_sem.at[0], recv, me, t).wait_recv()

    def at(zz, aa, bb):
        return (zz * na + aa) * nb + bb

    own_basis = basis_ref.at[:, pl.ds(pl.multiple_of(half * rank_half, rank_half), rank_half)]
    loads = [
        pltpu.make_async_copy(own_basis.at[: rows // 2], ball.at[me, 0], load_sem.at[0]),
        pltpu.make_async_copy(own_basis.at[rows // 2 :], ball.at[me, 1], load_sem.at[1]),
        pltpu.make_async_copy(inputs_ref, xv, load_sem.at[2]),
        pltpu.make_async_copy(cot_ref, cv, load_sem.at[3]),
        pltpu.make_async_copy(first_ref, fv, load_sem.at[4]),
        pltpu.make_async_copy(second_ref, sv, load_sem.at[5]),
        pltpu.make_async_copy(basis_ref, bv, load_sem.at[6]),
    ]

    barrier = pltpu.get_barrier_semaphore()
    for d in range(1, nz):
        pl.semaphore_signal(barrier, inc=1, device_id=((z + d) % nz * nq + q, t), device_id_type=MESH)
    for d in range(1, nq):
        pl.semaphore_signal(barrier, inc=1, device_id=(z * nq + (q + d) % nq, t), device_id_type=MESH)
    for d in range(1, tp):
        pl.semaphore_signal(barrier, inc=1, device_id=(me, (t + d) % tp), device_id_type=MESH)
    for load in loads:
        load.start()
    pl.semaphore_wait(barrier, nz - 1 + nq - 1 + tp - 1)

    class Gather:
        def __init__(self, view, recv, order):
            self.view, self.recv, self.order = view, recv, order

        def pass_on(self, c, fs):
            send(self.view(c), self.view(c), self.recv.at[c], fs, t)

        def near(self, k):
            c = at((z + k) % nz, a, b)
            if k > 0:
                arrive(self.view(c), self.recv.at[c])
            for d in range(1, na):
                self.pass_on(c, at(z, (a + d) % na, b))
            for d in range(1, nb):
                self.pass_on(c, at(z, a, (b + d) % nb))

        def begin(self):
            for d in range(1, nz):
                self.pass_on(me, at((z + d) % nz, a, b))
            self.near(0)

        def across(self, k):
            zz = (z + k) % nz
            if self.order == 0:
                for d in range(1, na):
                    c = at(zz, (a + d) % na, b)
                    arrive(self.view(c), self.recv.at[c])
                    for e in range(1, nb):
                        self.pass_on(c, at(z, a, (b + e) % nb))
            else:
                for e in range(1, nb):
                    c = at(zz, a, (b + e) % nb)
                    arrive(self.view(c), self.recv.at[c])
                    for d in range(1, na):
                        self.pass_on(c, at(z, (a + d) % na, b))

        def end(self, k):
            zz = (z + k) % nz
            for d in range(na):
                for e in range(nb):
                    seen = e == 0 if self.order == 0 else d == 0
                    if not seen:
                        c = at(zz, (a + d) % na, (b + e) % nb)
                        arrive(self.view(c), self.recv.at[c])

        def middle(self):
            for k in range(1, nz):
                self.near(k)
                self.across(k - 1)
            self.across(nz - 1)

    pieces = [
        Gather(lambda c, i=i: ball.at[c, i], b_recv.at[i], i) for i in range(2)
    ]
    loads[0].wait()
    loads[1].wait()
    for piece in pieces:
        piece.begin()
    for k in range(1, nz + 1):
        for piece in pieces:
            if k < nz:
                piece.near(k)
        for piece in pieces:
            piece.across(k - 1)
    loads[2].wait()
    projected = jnp.zeros((xv.shape[0], rank_half), jnp.float32)
    for k in range(nz):
        for piece in pieces:
            piece.end(k)
        zz = (z + k) % nz
        depth = nq * rows
        projected += jnp.dot(
            xv[:, pl.ds(pl.multiple_of(zz * depth, depth), depth)],
            ball[pl.ds(zz * nq, nq)].reshape(depth, rank_half),
            preferred_element_type=jnp.float32,
        )
    pbuf[half] = projected
    send(pbuf.at[half], pbuf.at[half], p_recv, me, partner)
    loads[3].wait()

    def shares(hh, slot, g):
        high, low = split2(pbuf[hh])
        cot = cv[:, g * width : (g + 1) * width]
        value = lax.dot_general(high, cot, CONTRACT, preferred_element_type=jnp.float32)
        value += lax.dot_general(low, cot, CONTRACT, preferred_element_type=jnp.float32)
        for k in range(nzh):
            for j in range(nq):
                row = (k * nq + j) * rr
                part[g, j, hh * nzh + k] = value[row : row + rr]
        for d in range(1, nq):
            to = (q + d) % nq
            send(
                part.at[g, to, pl.ds(hh * nzh, nzh)], rbuf.at[g, q, pl.ds(hh * nzh, nzh)],
                r_recv.at[g, slot, q], z * nq + to, t,
            )

    def combine(hh, slot, g):
        for d in range(1, nq):
            j = (q + d) % nq
            arrive(rbuf.at[g, j, pl.ds(hh * nzh, nzh)], r_recv.at[g, slot, j])
        for k in range(nzh):
            zz = hh * nzh + k
            total = part[g, q, zz]
            for d in range(1, nq):
                total += rbuf[g, (q + d) % nq, zz]
            zsend[g, zz] = total

            @pl.when(zz != z)
            def _():
                remote(
                    zsend.at[g, zz], zbuf.at[g, z], z_send.at[g, zz], z_recv.at[g, z], zz * nq + q, t
                ).start()

    def settle(g):
        low = zsend[g, z]
        for d in range(1, nz):
            zz = (z + d) % nz
            arrive(zbuf.at[g, zz], z_recv.at[g, zz])
            low += zbuf[g, zz]
        if g == 0:
            for load in loads[4:]:
                load.wait()
        here = slice(g * width, (g + 1) * width)
        first_new, second_new = moments(fv[:, here], sv[:, here], low)
        ubuf[g, me] = first_new / jnp.sqrt(second_new)
        low_ref[:, here] = low

    other = 1 - half
    updates = [
        Gather(lambda c, g=g: ubuf.at[g, c], u_recv.at[g], g % 2) for g in range(groups)
    ]
    for g in range(groups):
        shares(half, 0, g)
        if g == 0:
            arrive(pbuf.at[other], p_recv)
        shares(other, 1, g)
    for g in range(groups):
        combine(half, 0, g)
        if g > 0:
            settle(g - 1)
            updates[g - 1].begin()
        combine(other, 1, g)
        if g > 0:
            updates[g - 1].middle()
    settle(groups - 1)
    updates[groups - 1].begin()
    updates[groups - 1].middle()

    squares = []
    for g in range(groups):
        for k in range(nz):
            updates[g].end(k)
        if rr % 8 == 0:
            update = ubuf[g].reshape(rank, width)
        else:
            for i in range(n):
                ufull[i * rr : (i + 1) * rr, :] = ubuf[g, i]
            update = ufull[...]
        squares.append(jnp.sum(update * update, axis=0, keepdims=True))
        if g == groups - 1:
            total = sum(jnp.sum(x, axis=1, keepdims=True) for x in squares)
            sums[t] = jnp.broadcast_to(total, sums.shape[1:])
            for d in range(1, tp):
                send(sums.at[t], sums.at[t], s_recv.at[t], me, (t + d) % tp)
        high, rest = split2(update)
        product = jnp.dot(bv[...], high, preferred_element_type=jnp.float32)
        product += jnp.dot(bv[...], rest, preferred_element_type=jnp.float32)
        product_ref[:, g * width : (g + 1) * width] = product

    whole = sums[t][:1]
    for d in range(1, tp):
        c = (t + d) % tp
        arrive(sums.at[c], s_recv.at[c])
        whole += sums[c][:1]
    whole = whole / (rank * cols * tp)
    for g in range(groups):
        for i in range(width // DQK):
            head = jnp.sum(squares[g][:, i * DQK : (i + 1) * DQK], axis=1, keepdims=True)
            factor = 1.0 / jnp.sqrt(head / (rank * DQK) + whole)
            spot = slice(g * width + i * DQK, g * width + (i + 1) * DQK)
            factor_ref[:, spot] = jnp.broadcast_to(factor, (factor_ref.shape[0], DQK))

    for copy in started:
        copy.wait_send()
    for g in range(groups):
        for d in range(1, nz):
            zz = (z + d) % nz
            remote(
                zsend.at[g, zz], zbuf.at[g, z], z_send.at[g, zz], z_recv.at[g, z], zz * nq + q, t
            ).wait_send()


def finish(
    product_ref, factor_ref, low_ref, first_ref, second_ref, master_ref,
    step_ref, first_out, second_out, copy_ref,
):
    first_out[...], second_out[...] = moments(first_ref[...], second_ref[...], low_ref[...])
    step = product_ref[...] * factor_ref[:1]
    step_ref[...] = step
    copy_ref[...] = (master_ref[...] + step).astype(jnp.bfloat16)


def body(n, tp, inputs, query_cot, query_basis, query_master, query_first, query_second):
    nq = 1
    while nq * nq < n:
        nq *= 2
    nz = n // nq
    na = min(2, nq)
    nb = nq // na
    tokens, width = inputs.shape
    rows, rank = query_basis.shape
    rr, cols = query_first.shape
    groups = 2 if cols % (2 * DQK) == 0 else 1
    width_g = cols // groups
    sends = (2 + groups) * (nz + nz * nq) + 2 * groups * nq + tp
    f32, bf16 = jnp.float32, jnp.bfloat16
    dma = pltpu.SemaphoreType.DMA
    vmem = pl.BlockSpec(memory_space=pltpu.VMEM)
    hbm = pl.BlockSpec(memory_space=pl.ANY)
    product, factor, low = pl.pallas_call(
        functools.partial(kernel, n, na, nb, nz, tp, groups),
        out_shape=(
            jax.ShapeDtypeStruct((rows, cols), f32),
            jax.ShapeDtypeStruct((8, cols), f32),
            jax.ShapeDtypeStruct((rr, cols), f32),
        ),
        in_specs=[hbm] * 5,
        out_specs=(vmem,) * 3,
        scratch_shapes=[
            pltpu.VMEM((tokens, width), bf16),
            pltpu.VMEM((tokens, cols), bf16),
            pltpu.VMEM((rows, rank), bf16),
            pltpu.VMEM((rr, cols), f32),
            pltpu.VMEM((rr, cols), f32),
            pltpu.VMEM((n, 2, rows // 2, rank // 2), bf16),
            pltpu.VMEM((2, tokens, rank // 2), f32),
            pltpu.VMEM((groups, nq, nz, rr, width_g), f32),
            pltpu.VMEM((groups, nq, nz, rr, width_g), f32),
            pltpu.VMEM((groups, nz, rr, width_g), f32),
            pltpu.VMEM((groups, nz, rr, width_g), f32),
            pltpu.VMEM((groups, n, rr, width_g), f32),
            pltpu.VMEM((rank, width_g), f32),
            pltpu.VMEM((tp, 8, 128), f32),
            dma((7,)), dma((sends,)),
            dma, dma((2, n)), dma((groups, 2, nq)),
            dma((groups, nz)), dma((groups, nz)),
            dma((groups, n)), dma((tp,)),
        ],
        compiler_params=pltpu.CompilerParams(collective_id=0, has_side_effects=True),
    )(inputs, query_cot, query_basis, query_first, query_second)
    return pl.pallas_call(
        finish,
        out_shape=(
            jax.ShapeDtypeStruct((rows, cols), f32),
            jax.ShapeDtypeStruct((rr, cols), f32),
            jax.ShapeDtypeStruct((rr, cols), f32),
            jax.ShapeDtypeStruct((rows, cols), bf16),
        ),
        in_specs=[vmem] * 6,
        out_specs=(vmem,) * 4,
    )(product, factor, low, query_first, query_second, query_master)


def solution(mesh):
    placed = (
        P("fs", None),
        P("fs", "tp"),
        P("fs", None),
        P("fs", "tp"),
        P("fs", "tp"),
        P("fs", "tp"),
    )
    return jax.shard_map(
        functools.partial(body, mesh.shape["fs"], mesh.shape["tp"]),
        mesh=mesh,
        in_specs=placed,
        out_specs=(P("fs", "tp"),) * 4,
        check_vma=False,
    )
```

time: 39.8 us -> 53.1 us (1.33)
  Pallas kernels: 38.9 us -> 52.3 us
    pallas_call x1, Pallas kernels: 37 us -> 50.4 us  [body(): pl.pallas_call(functools.partial(kernel, n, na, nb, nz, tp, groups), out_...]
where the time goes in v3:
time: 53.1 us; the launch traced here: 52.9 us
  Pallas kernels  52.3 us (98%)
  between operations  0.64 us (1%)
    pallas_call x1, Pallas kernels, body(): pl.pallas_call(functools.partial(kernel, n, na, nb, nz, tp, groups), out_...  50.4 us
    pallas_call x1, Pallas kernels, body(): pl.pallas_call(finish, out_shape=(jax.ShapeDtypeStruct((rows, cols), f32)...  1.88 us

profile of v3, /device:TPU:0, one launch (start us, length us, event | category | flops | bytes accessed | tf_op | source)
XLA Modules:
  0.0 52.9 jit_solution(3363849896872918797)
XLA Ops:
  0.6 50.4 %shard_map.93 = (f32[128,512]{1,0:T(8,128)}, f32[8,512]{1,0:T(8,128)}, f32[16,512]{1,0:T(8,128)}) custom-call(bf16[256,2048]{1,0:T(8,128)(2,1)} %inputs_ref.1, bf16[256,512]{1,0:T(8,128)(2,1)} %cot_ref.1, bf16[128,256]{1,0:T(8,128)(2,1)} %basis_ref.1, f32[16,512]{1,0:T(8,128)} %first_ref.3, f32[16,512]{1,0:T(8,128)} %second_ref.3), custom_call_target="tpu_custom_call" | custom-call | tf_op jit(solution)/shard_map/pallas_call | solution.py:305
  51.1 1.9 %shard_map.94 = (f32[128,512]{1,0:T(8,128)}, f32[16,512]{1,0:T(8,128)}, f32[16,512]{1,0:T(8,128)}, bf16[128,512]{1,0:T(8,128)(2,1)}) custom-call(f32[128,512]{1,0:T(8,128)} %get-tuple-element.7.product_ref, f32[8,512]{1,0:T(8,128)} %get-tuple-element.8.factor_ref, f32[16,512]{1,0:T(8,128)} %get-tuple-element.9.low_ref, f32[16,512]{1,0:T(8,128)} %first_ref.3, ...), custom_call_target="tpu_custom_call" | custom-call | tf_op jit(solution)/shard_map/pallas_call | solution.py:336

commit v4 on v3

--- a/solution.py
+++ b/solution.py
@@ -94,10 +94,8 @@
             c = at((z + k) % nz, a, b)
             if k > 0:
                 arrive(self.view(c), self.recv.at[c])
-            for d in range(1, na):
-                self.pass_on(c, at(z, (a + d) % na, b))
-            for d in range(1, nb):
-                self.pass_on(c, at(z, a, (b + d) % nb))
+            for d in range(1, nq):
+                self.pass_on(c, z * nq + (q + d) % nq)
 
         def begin(self):
             for d in range(1, nz):
@@ -105,25 +103,13 @@
             self.near(0)
 
         def across(self, k):
-            zz = (z + k) % nz
-            if self.order == 0:
-                for d in range(1, na):
-                    c = at(zz, (a + d) % na, b)
-                    arrive(self.view(c), self.recv.at[c])
-                    for e in range(1, nb):
-                        self.pass_on(c, at(z, a, (b + e) % nb))
-            else:
-                for e in range(1, nb):
-                    c = at(zz, a, (b + e) % nb)
-                    arrive(self.view(c), self.recv.at[c])
-                    for d in range(1, na):
-                        self.pass_on(c, at(z, (a + d) % na, b))
+            pass
 
         def end(self, k):
             zz = (z + k) % nz
             for d in range(na):
                 for e in range(nb):
-                    seen = e == 0 if self.order == 0 else d == 0
+                    seen = d == 0 and e == 0
                     if not seen:
                         c = at(zz, (a + d) % na, (b + e) % nb)
                         arrive(self.view(c), self.recv.at[c])
@@ -295,7 +281,7 @@
     tokens, width = inputs.shape
     rows, rank = query_basis.shape
     rr, cols = query_first.shape
-    groups = 2 if cols % (2 * DQK) == 0 else 1
+    groups = 1
     width_g = cols // groups
     sends = (2 + groups) * (nz + nz * nq) + 2 * groups * nq + tp
     f32, bf16 = jnp.float32, jnp.bfloat16

time: 53.1 us -> 39.6 us (0.75)
  Pallas kernels: 52.3 us -> 38.7 us
    pallas_call x1, Pallas kernels: 50.4 us -> 36.8 us  [body(): pl.pallas_call(functools.partial(kernel, n, na, nb, nz, tp, groups), out_...]
where the time goes in v4:
time: 39.6 us; the launch traced here: 39.3 us
  Pallas kernels  38.7 us (98%)
  between operations  0.64 us (2%)
    pallas_call x1, Pallas kernels, body(): pl.pallas_call(functools.partial(kernel, n, na, nb, nz, tp, groups), out_...  36.8 us
    pallas_call x1, Pallas kernels, body(): pl.pallas_call(finish, out_shape=(jax.ShapeDtypeStruct((rows, cols), f32)...  1.88 us

profile of v4, /device:TPU:0, one launch (start us, length us, event | category | flops | bytes accessed | tf_op | source)
XLA Modules:
  0.0 39.3 jit_solution(9579433567683452713)
XLA Ops:
  0.6 36.8 %shard_map.93 = (f32[128,512]{1,0:T(8,128)}, f32[8,512]{1,0:T(8,128)}, f32[16,512]{1,0:T(8,128)}) custom-call(bf16[256,2048]{1,0:T(8,128)(2,1)} %inputs_ref.1, bf16[256,512]{1,0:T(8,128)(2,1)} %cot_ref.1, bf16[128,256]{1,0:T(8,128)(2,1)} %basis_ref.1, f32[16,512]{1,0:T(8,128)} %first_ref.3, f32[16,512]{1,0:T(8,128)} %second_ref.3), custom_call_target="tpu_custom_call" | custom-call | tf_op jit(solution)/shard_map/pallas_call | solution.py:291
  37.4 1.9 %shard_map.94 = (f32[128,512]{1,0:T(8,128)}, f32[16,512]{1,0:T(8,128)}, f32[16,512]{1,0:T(8,128)}, bf16[128,512]{1,0:T(8,128)(2,1)}) custom-call(f32[128,512]{1,0:T(8,128)} %get-tuple-element.7.product_ref, f32[8,512]{1,0:T(8,128)} %get-tuple-element.8.factor_ref, f32[16,512]{1,0:T(8,128)} %get-tuple-element.9.low_ref, f32[16,512]{1,0:T(8,128)} %first_ref.3, ...), custom_call_target="tpu_custom_call" | custom-call | tf_op jit(solution)/shard_map/pallas_call | solution.py:322

commit v5 on v4

--- a/solution.py
+++ b/solution.py
@@ -26,7 +26,7 @@
     n, na, nb, nz, tp, groups,
     inputs_ref, cot_ref, basis_ref, first_ref, second_ref,
     product_ref, factor_ref, low_ref,
-    xv, cv, bv, fv, sv, ball, pbuf, part, rbuf, zsend, zbuf, ubuf, ufull, sums,
+    xv, cv, bv, fv, sv, ball, pbuf, part, rbuf, zsend, zbuf, ubuf, ufull, uhigh, urest, sums,
     load_sem, send_sem, p_recv, b_recv, r_recv, z_send, z_recv, u_recv, s_recv,
 ):
     me = lax.axis_index("fs")
@@ -219,23 +219,28 @@
 
     squares = []
     for g in range(groups):
+        depth = nq * rr
+        square = jnp.zeros((1, width), jnp.float32)
         for k in range(nz):
             updates[g].end(k)
-        if rr % 8 == 0:
-            update = ubuf[g].reshape(rank, width)
-        else:
-            for i in range(n):
-                ufull[i * rr : (i + 1) * rr, :] = ubuf[g, i]
-            update = ufull[...]
-        squares.append(jnp.sum(update * update, axis=0, keepdims=True))
+            zz = (z + k) % nz
+            if rr % 8 == 0:
+                update = ubuf[g, pl.ds(zz * nq, nq)].reshape(depth, width)
+            else:
+                for i in range(nq):
+                    ufull[i * rr : (i + 1) * rr, :] = ubuf[g, zz * nq + i]
+                update = ufull[:depth, :]
+            square += jnp.sum(update * update, axis=0, keepdims=True)
+            spot = pl.ds(pl.multiple_of(zz * depth, depth), depth)
+            uhigh[spot, :], urest[spot, :] = split2(update)
+        squares.append(square)
         if g == groups - 1:
             total = sum(jnp.sum(x, axis=1, keepdims=True) for x in squares)
             sums[t] = jnp.broadcast_to(total, sums.shape[1:])
             for d in range(1, tp):
                 send(sums.at[t], sums.at[t], s_recv.at[t], me, (t + d) % tp)
-        high, rest = split2(update)
-        product = jnp.dot(bv[...], high, preferred_element_type=jnp.float32)
-        product += jnp.dot(bv[...], rest, preferred_element_type=jnp.float32)
+        product = jnp.dot(bv[...], uhigh[...], preferred_element_type=jnp.float32)
+        product += jnp.dot(bv[...], urest[...], preferred_element_type=jnp.float32)
         product_ref[:, g * width : (g + 1) * width] = product
 
     whole = sums[t][:1]
@@ -311,6 +316,8 @@
             pltpu.VMEM((groups, nz, rr, width_g), f32),
             pltpu.VMEM((groups, n, rr, width_g), f32),
             pltpu.VMEM((rank, width_g), f32),
+            pltpu.VMEM((rank, width_g), bf16),
+            pltpu.VMEM((rank, width_g), bf16),
             pltpu.VMEM((tp, 8, 128), f32),
             dma((7,)), dma((sends,)),
             dma, dma((2, n)), dma((groups, 2, nq)),

time: 39.6 us -> 39.6 us (level)
  no operation moved by 1% of the time
where the time goes in v5:
time: 39.6 us; the launch traced here: 39.3 us
  Pallas kernels  38.6 us (97%)
  between operations  0.64 us (2%)
    pallas_call x1, Pallas kernels, body(): pl.pallas_call(functools.partial(kernel, n, na, nb, nz, tp, groups), out_...  36.7 us
    pallas_call x1, Pallas kernels, body(): pl.pallas_call(finish, out_shape=(jax.ShapeDtypeStruct((rows, cols), f32)...  1.88 us

profile of v5, /device:TPU:0, one launch (start us, length us, event | category | flops | bytes accessed | tf_op | source)
XLA Modules:
  0.0 39.3 jit_solution(6165232038000535284)
XLA Ops:
  0.6 36.7 %shard_map.93 = (f32[128,512]{1,0:T(8,128)}, f32[8,512]{1,0:T(8,128)}, f32[16,512]{1,0:T(8,128)}) custom-call(bf16[256,2048]{1,0:T(8,128)(2,1)} %inputs_ref.1, bf16[256,512]{1,0:T(8,128)(2,1)} %cot_ref.1, bf16[128,256]{1,0:T(8,128)(2,1)} %basis_ref.1, f32[16,512]{1,0:T(8,128)} %first_ref.3, f32[16,512]{1,0:T(8,128)} %second_ref.3), custom_call_target="tpu_custom_call" | custom-call | tf_op jit(solution)/shard_map/pallas_call | solution.py:296
  37.4 1.9 %shard_map.94 = (f32[128,512]{1,0:T(8,128)}, f32[16,512]{1,0:T(8,128)}, f32[16,512]{1,0:T(8,128)}, bf16[128,512]{1,0:T(8,128)(2,1)}) custom-call(f32[128,512]{1,0:T(8,128)} %get-tuple-element.7.product_ref, f32[8,512]{1,0:T(8,128)} %get-tuple-element.8.factor_ref, f32[16,512]{1,0:T(8,128)} %get-tuple-element.9.low_ref, f32[16,512]{1,0:T(8,128)} %first_ref.3, ...), custom_call_target="tpu_custom_call" | custom-call | tf_op jit(solution)/shard_map/pallas_call | solution.py:329
